TPU v7x, 32 devices: a whole 2x2x4 slice. The times are simulated.
32 devices in a mesh: grp: 2 (over y), fs: 4 (over z), tp: 4 (over x, core).
Axes of the slice: x: 2, y: 2, z: 4, core: 2. Of those that a mesh axis runs over, the one named last changes fastest.
Arguments:
- tokens: bfloat16 [4096, 2048], P(('grp', 'fs')), parts along dimension 0, may hold values from -6 to 6
- norm_in: bfloat16 [2048], replicated, may hold values from 0.099609375 to 1.8984375
- w_value: bfloat16 [2048, 2048], P('fs', 'tp'), may hold values from -0.125 to 0.125
- w_gate: bfloat16 [2048, 2048], P('fs', 'tp'), may hold values from -0.125 to 0.125
- conv_kernel: float32 [31, 2048], replicated, as said below
- ln_gain: bfloat16 [2048], replicated, may hold values from 0.099609375 to 1.8984375
- ln_shift: bfloat16 [2048], replicated, may hold values from -3 to 3
- w_out: bfloat16 [2048, 2048], P('tp', 'fs'), may hold values from -0.125 to 0.125
- norm_mlp: bfloat16 [2048], replicated, may hold values from 0.099609375 to 1.8984375
- w_up: bfloat16 [2048, 8192], P('fs', 'tp'), may hold values from -0.125 to 0.125
- w_down: bfloat16 [8192, 2048], P('tp', 'fs'), may hold values from -0.0625 to 0.0625
Outputs:
- layer_out: bfloat16 [4096, 2048], P(('grp', 'fs', 'tp')), parts along dimension 0
There are 2 independent parts, one for each index of `grp`. A program takes and returns all parts, laid end to end along the dimension named above; an argument that names none is the same for every part. Nothing has to cross between parts.
Inputs may be any that keep to these rules, and one draw needn't show every extreme that they name: `conv_kernel`: a depthwise kernel.
All inputs are finite; a program needn't handle non-finite values.
Results may differ from a plain program's by a relative error of at most 0.018.
Values may be sent and summed in bfloat16 or wider, within the bound.
A program may use at most 64 MiB of HBM per device.

v0:
```python
import jax
import jax.numpy as jnp
from jax import lax
from jax.sharding import PartitionSpec as P

D = 2048
KERNEL = 31


def rms_scale(values, gain):
    as_float = values.astype(jnp.float32)
    scaled = as_float * lax.rsqrt(jnp.mean(as_float * as_float, axis=-1, keepdims=True) + 1e-06)
    return scaled * gain.astype(jnp.float32)


def shards(
    tokens, norm_in, w_value, w_gate, conv_kernel, ln_gain, ln_shift, w_out, norm_mlp, w_up, w_down
):
    seq_len = tokens.shape[0]
    col_width = w_value.shape[1]
    offset = lax.axis_index("tp") * col_width
    row_share = seq_len // lax.axis_size("tp")
    own_start = lax.axis_index("tp") * row_share
    normed_in = rms_scale(tokens, norm_in).astype(jnp.bfloat16)
    columns = normed_in
    values_f = jnp.dot(
        columns,
        lax.all_gather(w_value, "fs", axis=0, tiled=True),
        preferred_element_type=jnp.float32,
    )
    gate_act = jnp.dot(
        columns,
        lax.all_gather(w_gate, "fs", axis=0, tiled=True),
        preferred_element_type=jnp.float32,
    )
    gated = values_f * jax.nn.sigmoid(gate_act)
    kernel = lax.dynamic_slice_in_dim(conv_kernel, offset, col_width, 1)
    padded = jnp.pad(gated, ((KERNEL - 1, 0), (0, 0)))
    convolved = jnp.zeros_like(gated)
    for tap_index in range(KERNEL):
        convolved = convolved + kernel[tap_index][None, :] * padded[tap_index : tap_index + seq_len]
    stats = lax.psum((jnp.sum(convolved, axis=1), jnp.sum(convolved * convolved, axis=1)), "tp")
    chan_mean = (stats[0] / D)[:, None]
    chan_msq = (stats[1] / D)[:, None]
    variance = chan_msq - chan_mean * chan_mean
    gain_part = lax.dynamic_slice_in_dim(ln_gain, offset, col_width, 0).astype(jnp.float32)
    shift_part = lax.dynamic_slice_in_dim(ln_shift, offset, col_width, 0).astype(jnp.float32)
    normed = (convolved - chan_mean) * lax.rsqrt(variance + 1e-05) * gain_part + shift_part
    activated = jax.nn.silu(normed).astype(jnp.bfloat16)
    partial_value = jnp.dot(
        activated,
        lax.all_gather(w_out, "fs", axis=1, tiled=True),
        preferred_element_type=jnp.float32,
    )
    mixed = lax.psum(partial_value.astype(jnp.bfloat16), "tp").astype(jnp.float32)
    residual = tokens.astype(jnp.float32) + mixed
    normed_mlp = rms_scale(residual, norm_mlp).astype(jnp.bfloat16)
    residual_own = lax.dynamic_slice_in_dim(residual, own_start, row_share, 0)
    columns = normed_mlp
    up_act = jnp.dot(
        columns, lax.all_gather(w_up, "fs", axis=0, tiled=True), preferred_element_type=jnp.float32
    )
    hidden = jnp.square(jax.nn.relu(up_act)).astype(jnp.bfloat16)
    whole_down = lax.all_gather(w_down, "fs", axis=1, tiled=True)
    mlp_own = lax.psum_scatter(
        jnp.dot(hidden, whole_down, preferred_element_type=jnp.float32).astype(jnp.bfloat16),
        "tp",
        scatter_dimension=0,
        tiled=True,
    ).astype(jnp.float32)
    return (residual_own + mlp_own).astype(jnp.bfloat16)


def solution(mesh):
    in_specs = (
        P(("grp", "fs"), None),
        P(),
        P("fs", "tp"),
        P("fs", "tp"),
        P(),
        P(),
        P(),
        P("tp", "fs"),
        P(),
        P("fs", "tp"),
        P("tp", "fs"),
    )
    out_specs = P(("grp", "fs", "tp"), None)
    return jax.shard_map(shards, mesh=mesh, in_specs=in_specs, out_specs=out_specs, check_vma=False)
```

profile of v0, /device:TPU:0, one launch (start us, length us, event | category | flops | bytes accessed | tf_op | source)
XLA Modules:
  0.0 559.9 jit_solution(14983291080787817863)
XLA Ops:
  6.5 0.0 copy-start
  6.5 0.0 all-gather.8.cloned.1.call-start
  6.5 0.7 all-gather.8.cloned.1.call-update
  7.3 0.0 all-gather.6.cloned.1.call-start
  7.3 0.7 all-gather.6.cloned.1.call-update
  8.0 0.0 all-gather.10.cloned.1.call-start
  8.1 0.7 all-gather.10.cloned.1.call-update
  8.7 0.0 all-reduce.4.cloned.1.call-start
  8.8 0.7 convert_element_type.46
  9.5 0.8 dynamic-slice_convert_fusion
  10.3 1.1 fusion.50
  11.4 1.4 constant_dynamic-slice_fusion
  12.8 2.1 fusion
  14.8 42.5 %all-gather.8.cloned.1.call-done = bf16[2048,512]{1,0:T(8,128)(2,1)} async-done(((bf16[512,512]{1,0:T(8,128)(2,1)}), bf16[2048,512]{1,0:T(8,128)(2,1)}) %all-gather.8.cloned.1.call-update) | async-done | bytes 2097168 | tf_op jit(solution)/shard_map/all_gather | solution.py:33
  57.3 0.0 copy-done
  57.3 3.0 fusion.7
  60.4 43.0 %all-gather.6.cloned.1.call-done = bf16[2048,512]{1,0:T(8,128)(2,1)} async-done(((bf16[512,512]{1,0:T(8,128)(2,1)}), bf16[2048,512]{1,0:T(8,128)(2,1)}) %all-gather.6.cloned.1.call-update) | async-done | bytes 2097168 | tf_op jit(solution)/shard_map/all_gather | solution.py:28
  103.4 2.9 convolution_multiply_fusion
  106.3 5.0 fusion.49
  111.3 6.8 %all-reduce.1 = (f32[512]{0:T(512)S(1)}, f32[512]{0:T(512)S(1)}) all-reduce(f32[512]{0:T(512)S(1)} %get-tuple-element.6, f32[512]{0:T(512)S(1)} %get-tuple-element.5), channel_id=1, replica_groups=mesh['grp'=2,'fs'=4,'tp'=4] {'tp'}, use_global_device_ids=true, to_apply=%region_4.5 | all-reduce | flops 1024 | bytes 8192 | tf_op jit(solution)/shard_map/psum | solution.py:42
  118.1 31.4 %all-gather.10.cloned.1.call-done = bf16[512,2048]{1,0:T(8,128)(2,1)} async-done(((bf16[512,512]{1,0:T(8,128)(2,1)}), bf16[512,2048]{1,0:T(8,128)(2,1)}) %all-gather.10.cloned.1.call-update) | async-done | bytes 2097168 | tf_op jit(solution)/shard_map/all_gather | solution.py:52
  149.4 4.4 convolution_convert_fusion.1
  153.9 0.0 all-reduce.4.cloned.1.call-update
  153.9 0.0 copy-start.1
  153.9 0.0 all-gather.12.cloned.1.call-start
  153.9 0.5 all-gather.12.cloned.1.call-update
  154.5 0.0 all-gather.14.cloned.1.call-start
  154.5 0.5 all-gather.14.cloned.1.call-update
  155.1 0.2 reduce-scatter.2.cloned.1.call-start
  155.3 0.0 copy-done.1
  155.3 48.9 %all-reduce.4.cloned.1.call-done = bf16[512,2048]{1,0:T(8,128)(2,1)} async-done(((bf16[512,2048]{1,0:T(8,128)(2,1)}), bf16[512,2048]{1,0:T(8,128)(2,1)}) %all-reduce.4.cloned.1.call-update) | async-done | bytes 2097168 | tf_op jit(solution)/shard_map/psum | solution.py:55
  204.2 4.2 convert_add_fusion
  208.4 146.9 %all-gather.12.cloned.1.call-done = bf16[2048,2048]{1,0:T(8,128)(2,1)} async-done(((bf16[512,2048]{1,0:T(8,128)(2,1)}), bf16[2048,2048]{1,0:T(8,128)(2,1)}) %all-gather.12.cloned.1.call-update) | async-done | bytes 8388624 | tf_op jit(solution)/shard_map/all_gather | solution.py:61
  355.4 149.3 %all-gather.14.cloned.1.call-done = bf16[2048,2048]{1,0:T(8,128)(2,1)} async-done(((bf16[2048,512]{1,0:T(8,128)(2,1)}), bf16[2048,2048]{1,0:T(8,128)(2,1)}) %all-gather.14.cloned.1.call-update) | async-done | bytes 8388624 | tf_op jit(solution)/shard_map/all_gather | solution.py:64
  504.6 16.6 %convolution_convert_fusion = bf16[512,2048]{1,0:T(8,128)(2,1)} fusion(bf16[2048,2048]{1,0:T(8,128)(2,1)} %all-gather.14.cloned.1.call-done, bf16[2048,2048]{1,0:T(8,128)(2,1)} %all-gather.12.cloned.1.call-done, f32[2048]{0:T(1024)S(1)} %convert_element_type.53, f32[512]{0:T(512)S(1)} %add_rsqrt_fusion, bf16[512,2048]{1,0:T(8,128)(2,1)S(1)} %copy-done, ...), kind=kOutput, calls=%fused_computation.9 | convolution fusion | flops 8600420352 | bytes 23078912 | tf_op jit(solution)/shard_map/dot_general | solution.py:66
  521.2 0.0 reduce-scatter.2.cloned.1.call-update
  521.2 29.5 %reduce-scatter.2.cloned.1.call-done = bf16[128,2048]{1,0:T(8,128)(2,1)} async-done(((bf16[512,2048]{1,0:T(8,128)(2,1)}), bf16[128,2048]{1,0:T(8,128)(2,1)}) %reduce-scatter.2.cloned.1.call-update) | async-done | bytes 524304 | tf_op jit(solution)/shard_map/reduce_scatter | solution.py:65
  550.8 2.3 add_convert_fusion
  (4 shorter events, 0.0 us)
Async XLA Ops:
  6.5 50.8 %copy-start = (bf16[512,2048]{1,0:T(8,128)(2,1)S(1)}, bf16[512,2048]{1,0:T(8,128)(2,1)}, u32[]{:S(2)}) copy-start(bf16[512,2048]{1,0:T(8,128)(2,1)} %param.11) | copy-start | bytes 6291460
  6.5 50.8 %all-gather.8.cloned.1.call-start = ((), (), s32[]{:S(2)}) async-start(), calls=%async_computation.2 | async-start | bytes 2621440 | tf_op jit(solution)/shard_map/all_gather | solution.py:33
  7.3 96.1 %all-gather.6.cloned.1.call-start = ((), (), s32[]{:S(2)}) async-start(), calls=%async_computation.1 | async-start | bytes 2621440 | tf_op jit(solution)/shard_map/all_gather | solution.py:28
  8.0 141.4 %all-gather.10.cloned.1.call-start = ((), (), s32[]{:S(2)}) async-start(), calls=%async_computation.3 | async-start | bytes 2621440 | tf_op jit(solution)/shard_map/all_gather | solution.py:52
  8.7 195.5 %all-reduce.4.cloned.1.call-start = ((), (), s32[]{:S(2)}) async-start(), calls=%async_computation.4 | async-start | bytes 4194304 | tf_op jit(solution)/shard_map/psum | solution.py:55
  153.9 1.4 copy-start.1
  153.9 201.5 %all-gather.12.cloned.1.call-start = ((), (), s32[]{:S(2)}) async-start(), calls=%async_computation.5 | async-start | bytes 10485760 | tf_op jit(solution)/shard_map/all_gather | solution.py:61
  154.5 350.1 %all-gather.14.cloned.1.call-start = ((), (), s32[]{:S(2)}) async-start(), calls=%async_computation.6 | async-start | bytes 10485760 | tf_op jit(solution)/shard_map/all_gather | solution.py:64
  155.1 395.7 %reduce-scatter.2.cloned.1.call-start = ((), (), s32[]{:S(2)}) async-start(), calls=%async_computation.7 | async-start | bytes 2621440 | tf_op jit(solution)/shard_map/reduce_scatter | solution.py:65
Sparse Core Ops, SparseCore 0:
  8.9 48.3 all-gather.7
  58.9 44.4 all-gather.5
  105.0 44.4 all-gather.9
  154.0 50.1 all-reduce.3
  205.6 149.6 all-gather.11
  356.8 147.7 all-gather.13
  521.4 29.3 reduce-scatter.1
where the time goes:
time: 560 us
  waiting for transfers between devices  495 us (88%)
  matrix products  26.9 us (5%)
  other arithmetic  15 us (3%)
  between operations  13.6 us (2%)
  blocking collectives  6.79 us (1%)
    all_gather x1, waiting for transfers between devices, shards(): whole_down = lax.all_gather(w_down, 'fs', axis=1, tiled=True)  149 us
    all_gather x1, waiting for transfers between devices, shards(): lax.all_gather(w_up, 'fs', axis=0, tiled=True)  147 us
    psum x1, waiting for transfers between devices, shards(): lax.psum(partial_value.astype(jnp.bfloat16), 'tp').astype(jnp.float32)  48.9 us
    all_gather x1, waiting for transfers between devices, shards(): lax.all_gather(w_value, 'fs', axis=0, tiled=True)  43 us
    all_gather x1, waiting for transfers between devices, shards(): lax.all_gather(w_gate, 'fs', axis=0, tiled=True)  42.5 us
    all_gather x1, waiting for transfers between devices, shards(): lax.all_gather(w_out, 'fs', axis=1, tiled=True)  31.4 us
    reduce_scatter x1, waiting for transfers between devices, shards(): lax.psum_scatter(jnp.dot(hidden, whole_down, preferred_element_type=jnp.f...  29.5 us
    dot_general x1, matrix products, shards(): jnp.dot(hidden, whole_down, preferred_element_type=jnp.float32)  16.6 us
  transfers between devices with their start and end apart: 7, of which 7 were waited for; matrix products, arithmetic and copies ran while one was open for 4% of the time, Pallas kernels for 0%

commit v1 on v0

--- a/solution.py
+++ b/solution.py
@@ -61,7 +61,12 @@
         columns, lax.all_gather(w_up, "fs", axis=0, tiled=True), preferred_element_type=jnp.float32
     )
     hidden = jnp.square(jax.nn.relu(up_act)).astype(jnp.bfloat16)
-    whole_down = lax.all_gather(w_down, "fs", axis=1, tiled=True)
+    ring = [w_down]
+    for hop in range(3):
+        ring.append(lax.ppermute(ring[-1], "fs", [(dev, (dev + 1) % 4) for dev in range(4)]))
+    whole_down = jnp.roll(
+        jnp.concatenate(ring[::-1], axis=1), (lax.axis_index("fs") + 1) * ring[0].shape[1], axis=1
+    )
     mlp_own = lax.psum_scatter(
         jnp.dot(hidden, whole_down, preferred_element_type=jnp.float32).astype(jnp.bfloat16),
         "tp",

time: 560 us -> 505 us (0.902)
  waiting for transfers between devices: 495 us -> 392 us
  starting transfers between devices: 0.42 us -> 27.6 us
  local copies, waits for them, and re-layouts: 2.49 us -> 22.6 us
    ppermute x0 -> x3, waiting for transfers between devices: none -> 221 us  [shards(): lax.ppermute(ring[-1], 'fs', [(dev, (dev + 1) % 4) for dev in range(4)])]
    all_gather x1 -> x0, waiting for transfers between devices: 149 us -> none  [shards(): whole_down = lax.all_gather(w_down, 'fs', axis=1, tiled=True)]
    all_gather x1, waiting for transfers between devices: 147 us -> 6.69 us  [shards(): lax.all_gather(w_up, 'fs', axis=0, tiled=True)]
    psum x1, waiting for transfers between devices: 48.9 us -> 0.01 us  [shards(): lax.psum(partial_value.astype(jnp.bfloat16), 'tp').astype(jnp.float32)]
    ppermute x0 -> x3, starting transfers between devices: none -> 27.4 us  [shards(): lax.ppermute(ring[-1], 'fs', [(dev, (dev + 1) % 4) for dev in range(4)])]
    unnamed x4 -> x17, local copies, waits for them, and re-layouts: 0.01 us -> 18.6 us
    reduce_scatter x1, waiting for transfers between devices: 29.5 us -> 45.4 us  [shards(): lax.psum_scatter(jnp.dot(hidden, whole_down, preferred_element_type=jnp.f...]
  transfers between devices with their start and end apart: 7 -> 9, of which waited for: 7 -> 8; matrix products, arithmetic and copies ran while one was open for 4% -> 8% of each run, Pallas kernels for 0% -> 0%
where the time goes in v1:
time: 505 us
  waiting for transfers between devices  392 us (78%)
  starting transfers between devices  27.6 us (5%)
  matrix products  27.6 us (5%)
  local copies, waits for them, and re-layouts  22.6 us (4%)
  other arithmetic  15.1 us (3%)
  between operations  13.5 us (3%)
  blocking collectives  6.79 us (1%)
    ppermute x3, waiting for transfers between devices, shards(): lax.ppermute(ring[-1], 'fs', [(dev, (dev + 1) % 4) for dev in range(4)])  221 us
    reduce_scatter x1, waiting for transfers between devices, shards(): lax.psum_scatter(jnp.dot(hidden, whole_down, preferred_element_type=jnp.f...  45.4 us
    all_gather x1, waiting for transfers between devices, shards(): lax.all_gather(w_gate, 'fs', axis=0, tiled=True)  42.5 us
    all_gather x1, waiting for transfers between devices, shards(): lax.all_gather(w_value, 'fs', axis=0, tiled=True)  42.4 us
    all_gather x1, waiting for transfers between devices, shards(): lax.all_gather(w_out, 'fs', axis=1, tiled=True)  31.4 us
    ppermute x3, starting transfers between devices, shards(): lax.ppermute(ring[-1], 'fs', [(dev, (dev + 1) % 4) for dev in range(4)])  27.4 us
    unnamed x17, local copies, waits for them, and re-layouts  18.6 us
    dot_general x1, matrix products, shards(): jnp.dot(hidden, whole_down, preferred_element_type=jnp.float32)  16.5 us
  transfers between devices with their start and end apart: 9, of which 8 were waited for; matrix products, arithmetic and copies ran while one was open for 8% of the time, Pallas kernels for 0%

profile of v1, /device:TPU:0, one launch (start us, length us, event | category | flops | bytes accessed | tf_op | source)
XLA Modules:
  0.0 504.8 jit_solution(14855344243949360485)
XLA Ops:
  6.5 0.0 all-gather.7.cloned.1.call-start
  6.5 0.7 all-gather.7.cloned.1.call-update
  7.3 0.0 all-gather.5.cloned.1.call-start
  7.3 0.7 all-gather.5.cloned.1.call-update
  8.0 0.0 all-gather.9.cloned.1.call-start
  8.1 0.7 all-gather.9.cloned.1.call-update
  8.7 0.0 all-reduce.4.cloned.1.call-start
  8.8 0.7 convert_element_type.46
  9.5 0.8 dynamic-slice_convert_fusion
  10.3 1.1 fusion.57
  11.4 1.4 constant_dynamic-slice_fusion
  12.7 2.1 fusion.2
  14.8 0.0 copy-start
  14.8 42.5 %all-gather.7.cloned.1.call-done = bf16[2048,512]{1,0:T(8,128)(2,1)} async-done(((bf16[512,512]{1,0:T(8,128)(2,1)}), bf16[2048,512]{1,0:T(8,128)(2,1)}) %all-gather.7.cloned.1.call-update) | async-done | bytes 2097168 | tf_op jit(solution)/shard_map/all_gather | solution.py:33
  57.3 3.7 fusion.12
  61.0 42.4 %all-gather.5.cloned.1.call-done = bf16[2048,512]{1,0:T(8,128)(2,1)} async-done(((bf16[512,512]{1,0:T(8,128)(2,1)}), bf16[2048,512]{1,0:T(8,128)(2,1)}) %all-gather.5.cloned.1.call-update) | async-done | bytes 2097168 | tf_op jit(solution)/shard_map/all_gather | solution.py:28
  103.4 0.0 copy-done
  103.4 2.9 convolution_multiply_fusion
  106.3 5.0 fusion.56
  111.3 6.8 %all-reduce.1 = (f32[512]{0:T(512)S(1)}, f32[512]{0:T(512)S(1)}) all-reduce(f32[512]{0:T(512)S(1)} %get-tuple-element.6, f32[512]{0:T(512)S(1)} %get-tuple-element.5), channel_id=1, replica_groups=mesh['grp'=2,'fs'=4,'tp'=4] {'tp'}, use_global_device_ids=true, to_apply=%region_4.5 | all-reduce | flops 1024 | bytes 8192 | tf_op jit(solution)/shard_map/psum | solution.py:42
  118.1 31.4 %all-gather.9.cloned.1.call-done = bf16[512,2048]{1,0:T(8,128)(2,1)} async-done(((bf16[512,512]{1,0:T(8,128)(2,1)}), bf16[512,2048]{1,0:T(8,128)(2,1)}) %all-gather.9.cloned.1.call-update) | async-done | bytes 2097168 | tf_op jit(solution)/shard_map/all_gather | solution.py:52
  149.4 4.4 convolution_convert_fusion
  153.9 0.0 all-reduce.4.cloned.1.call-update
  153.9 0.0 all-gather.11.cloned.1.call-start
  154.0 0.5 all-gather.11.cloned.1.call-update
  154.5 0.0 reduce-scatter.2.cloned.1.call-start
  154.6 0.2 collective-permute-start
  154.8 49.0 %collective-permute-done = bf16[2048,512]{1,0:T(8,128)(2,1)S(1)} collective-permute-done((bf16[2048,512]{1,0:T(8,128)(2,1)}, bf16[2048,512]{1,0:T(8,128)(2,1)S(1)}, u32[]{:S(2)}, u32[]{:S(2)}) %collective-permute-start) | collective-permute-done | bytes 2097184 | tf_op jit(solution)/shard_map/ppermute | solution.py:66
  203.8 1.4 copy-done.2
  205.2 0.0 collective-permute-start.1
  205.2 84.0 %collective-permute-done.1 = bf16[2048,512]{1,0:T(8,128)(2,1)} collective-permute-done((bf16[2048,512]{1,0:T(8,128)(2,1)S(1)}, bf16[2048,512]{1,0:T(8,128)(2,1)}, u32[]{:S(2)}, u32[]{:S(2)}) %collective-permute-start.1) | collective-permute-done | bytes 2097184 | tf_op jit(solution)/shard_map/ppermute | solution.py:66
  289.3 27.2 %collective-permute-start.2 = (bf16[2048,512]{1,0:T(8,128)(2,1)}, bf16[2048,512]{1,0:T(8,128)(2,1)}, u32[]{:S(2)}, u32[]{:S(2)}) collective-permute-start(bf16[2048,512]{1,0:T(8,128)(2,1)} %collective-permute-done.1), channel_id=1, source_target_pairs={{0,4},{4,8},{8,12},{12,0},{1,5},{5,9},{9,13},{13,1},{2,6},{6,10},{... | collective-permute-start | bytes 6291464 | tf_op jit(solution)/shard_map/ppermute | solution.py:66
  316.4 0.0 copy-done.4
  316.4 4.2 convert_add_fusion
  320.7 87.5 %collective-permute-done.2 = bf16[2048,512]{1,0:T(8,128)(2,1)} collective-permute-done((bf16[2048,512]{1,0:T(8,128)(2,1)}, bf16[2048,512]{1,0:T(8,128)(2,1)}, u32[]{:S(2)}, u32[]{:S(2)}) %collective-permute-start.2) | collective-permute-done | bytes 2097184 | tf_op jit(solution)/shard_map/ppermute | solution.py:66
  408.2 3.1 constant_dynamic-update-slice_fusion.7
  411.3 3.3 constant_dynamic-update-slice_fusion.6
  414.6 1.6 constant_dynamic-update-slice_fusion.5
  416.2 1.5 constant_dynamic-update-slice_fusion.4
  417.7 3.1 constant_dynamic-update-slice_fusion.3
  420.8 3.1 constant_dynamic-update-slice_fusion.2
  423.9 1.5 constant_dynamic-update-slice_fusion.1
  425.5 1.5 constant_dynamic-update-slice_fusion
  427.0 6.7 %all-gather.11.cloned.1.call-done = bf16[2048,2048]{1,0:T(8,128)(2,1)} async-done(((bf16[512,2048]{1,0:T(8,128)(2,1)}), bf16[2048,2048]{1,0:T(8,128)(2,1)}) %all-gather.11.cloned.1.call-update) | async-done | bytes 8388624 | tf_op jit(solution)/shard_map/all_gather | solution.py:61
  433.7 16.5 %fusion.5 = bf16[512,2048]{1,0:T(8,128)(2,1)} fusion(bf16[2048,4096]{1,0:T(8,128)(2,1)} %constant_dynamic-update-slice_fusion, s32[]{:T(128)S(6)} %select_n.24, bf16[2048,2048]{1,0:T(8,128)(2,1)} %all-gather.11.cloned.1.call-done, f32[2048]{0:T(1024)S(1)} %convert_element_type.53, f32[512]{0:T(512)S(1)} %add_rsqrt_fusion, ...), kind=kOutput, calls=%fused_computation.11 | convolution fusion | flops 8600420352 | bytes 23078916 | tf_op jit(solution)/shard_map/dot_general | solution.py:71
  450.2 0.0 reduce-scatter.2.cloned.1.call-update
  450.3 45.4 %reduce-scatter.2.cloned.1.call-done = bf16[128,2048]{1,0:T(8,128)(2,1)} async-done(((bf16[512,2048]{1,0:T(8,128)(2,1)}), bf16[128,2048]{1,0:T(8,128)(2,1)}) %reduce-scatter.2.cloned.1.call-update) | async-done | bytes 524304 | tf_op jit(solution)/shard_map/reduce_scatter | solution.py:70
  495.7 2.3 add_convert_fusion
  (11 shorter events, 0.0 us)
Async XLA Ops:
  6.5 50.8 %all-gather.7.cloned.1.call-start = ((), (), s32[]{:S(2)}) async-start(), calls=%async_computation.2 | async-start | bytes 2621440 | tf_op jit(solution)/shard_map/all_gather | solution.py:33
  7.3 96.1 %all-gather.5.cloned.1.call-start = ((), (), s32[]{:S(2)}) async-start(), calls=%async_computation.1 | async-start | bytes 2621440 | tf_op jit(solution)/shard_map/all_gather | solution.py:28
  8.0 141.4 %all-gather.9.cloned.1.call-start = ((), (), s32[]{:S(2)}) async-start(), calls=%async_computation.3 | async-start | bytes 2621440 | tf_op jit(solution)/shard_map/all_gather | solution.py:52
  8.7 307.7 %all-reduce.4.cloned.1.call-start = ((), (), s32[]{:S(2)}) async-start(), calls=%async_computation.4 | async-start | bytes 4194304 | tf_op jit(solution)/shard_map/psum | solution.py:55
  14.8 88.6 %copy-start = (bf16[512,2048]{1,0:T(8,128)(2,1)S(1)}, bf16[512,2048]{1,0:T(8,128)(2,1)}, u32[]{:S(2)}) copy-start(bf16[512,2048]{1,0:T(8,128)(2,1)} %param.11) | copy-start | bytes 6291460
  153.9 162.5 %copy-start.4 = (bf16[2048]{0:T(1024)(128)(2,1)S(1)}, bf16[2048]{0:T(1024)(128)(2,1)}, u32[]{:S(2)}) copy-start(bf16[2048]{0:T(1024)(128)(2,1)} %param.19) | copy-start | bytes 12292
  153.9 279.8 %all-gather.11.cloned.1.call-start = ((), (), s32[]{:S(2)}) async-start(), calls=%async_computation.5 | async-start | bytes 10485760 | tf_op jit(solution)/shard_map/all_gather | solution.py:61
  154.5 341.2 %reduce-scatter.2.cloned.1.call-start = ((), (), s32[]{:S(2)}) async-start(), calls=%async_computation.6 | async-start | bytes 2621440 | tf_op jit(solution)/shard_map/reduce_scatter | solution.py:70
  154.6 49.3 %collective-permute-start = (bf16[2048,512]{1,0:T(8,128)(2,1)}, bf16[2048,512]{1,0:T(8,128)(2,1)S(1)}, u32[]{:S(2)}, u32[]{:S(2)}) collective-permute-start(bf16[2048,512]{1,0:T(8,128)(2,1)} %param.21), channel_id=1, source_target_pairs={{0,4},{4,8},{8,12},{12,0},{1,5},{5,9},{9,13},{13,1},{2,6},{6,10},{... | collective-permute-start | bytes 6291464 | tf_op jit(solution)/shard_map/ppermute | solution.py:66
  203.8 1.4 copy-start.2
  205.2 84.0 %collective-permute-start.1 = (bf16[2048,512]{1,0:T(8,128)(2,1)S(1)}, bf16[2048,512]{1,0:T(8,128)(2,1)}, u32[]{:S(2)}, u32[]{:S(2)}) collective-permute-start(bf16[2048,512]{1,0:T(8,128)(2,1)S(1)} %collective-permute-done), channel_id=1, source_target_pairs={{0,4},{4,8},{8,12},{12,0},{1,5},{5,9},{9,13},{13,1},{2,6},{6,10},{... | collective-permute-start | bytes 6291464 | tf_op jit(solution)/shard_map/ppermute | solution.py:66
  289.3 119.0 %collective-permute-start.2 = (bf16[2048,512]{1,0:T(8,128)(2,1)}, bf16[2048,512]{1,0:T(8,128)(2,1)}, u32[]{:S(2)}, u32[]{:S(2)}) collective-permute-start(bf16[2048,512]{1,0:T(8,128)(2,1)} %collective-permute-done.1), channel_id=1, source_target_pairs={{0,4},{4,8},{8,12},{12,0},{1,5},{5,9},{9,13},{13,1},{2,6},{6,10},{... | collective-permute-start | bytes 6291464 | tf_op jit(solution)/shard_map/ppermute | solution.py:66
  320.7 93.9 %copy-start.3 = (bf16[2048,512]{1,0:T(8,128)(2,1)S(1)}, bf16[2048,512]{1,0:T(8,128)(2,1)}, u32[]{:S(2)}) copy-start(bf16[2048,512]{1,0:T(8,128)(2,1)} %copy-done.2) | copy-start | bytes 6291460
  411.3 4.8 copy-start.1
Sparse Core Ops, SparseCore 0:
  8.9 48.3 all-gather.6
  58.9 44.4 all-gather.4
  105.0 44.4 all-gather.8
  154.0 50.1 all-reduce.3
  205.7 227.9 all-gather.10
  450.4 45.2 reduce-scatter.1
